TPU v7x, 32 devices: a whole 2x2x4 slice. The times are simulated.
32 devices in a mesh: sp: 16 (over z, y, core), tp: 2 (over x).
Axes of the slice: x: 2, y: 2, z: 4, core: 2. Of those that a mesh axis runs over, the one named last changes fastest.
Arguments:
- inputs: bfloat16 [4096, 4096], P('sp', 'tp'), may hold values from -20 to 20
- norm_gain: float32 [3, 4096], replicated, may hold values from 0.1 to 1.9
- in_weight: bfloat16 [3, 4096, 1024], P(None, 'tp', 'sp'), may hold values from -0.09375 to 0.09375
- pool_scale: float32 [3, 1024], replicated, may hold values from 0.1 to 1.9
- out_weight: bfloat16 [3, 1024, 4096], P(None, 'sp', 'tp'), may hold values from -0.1875 to 0.1875
Outputs:
- final_state: bfloat16 [4096, 4096], P('sp', 'tp')
All inputs are finite; a program needn't handle non-finite values.
Results may differ from a plain program's by a relative error of at most 0.017.
Values may be sent and summed in bfloat16 or wider, within the bound.
A program may use at most 64 MiB of HBM per device.

v0:
```python
import jax
import jax.numpy as jnp
from jax import lax
from jax.sharding import PartitionSpec as P

D = 4096
P_SIZE = 1024
LAYERS = 3
epsilon = 1e-06
halo_rows = 16
group_count = 4


def from_behind(value, axis, steps):
    count = lax.axis_size(axis)
    initial, last = (max(0, -steps), min(count, count - steps))
    return lax.ppermute(value, axis, [(source, source + steps) for source in range(initial, last)])


def window_means(extended, row_count, first_channel, first_pos, pool_total):
    width = extended.shape[1]
    channel = first_channel + lax.broadcasted_iota(jnp.int32, (1, width), 1)
    group_index = channel // (pool_total // group_count)
    window_len = jnp.left_shift(jnp.int32(2), group_index)
    running = jnp.zeros((row_count, width), jnp.float32)
    for offset in range(halo_rows):
        shifted = extended[halo_rows - offset : halo_rows - offset + row_count]
        running = running + jnp.where(offset < window_len, shifted, 0.0)
    position = first_pos + lax.broadcasted_iota(jnp.int32, (row_count, 1), 0)
    divisor = jnp.minimum(position + 1, window_len).astype(jnp.float32)
    return running / divisor - extended[halo_rows:]


def body(inputs, norm_gain, in_weight, pool_scale, out_weight):
    row_count, feature_part = inputs.shape
    channel_part = P_SIZE // lax.axis_size("tp")
    tp_index = lax.axis_index("tp")
    sp_index = lax.axis_index("sp")
    current = inputs
    in_all, out_all = (
        lax.all_gather(in_weight, "sp", axis=2, tiled=True),
        lax.all_gather(out_weight, "sp", axis=1, tiled=True),
    )
    for layer_index in range(LAYERS):
        gain_row = norm_gain[layer_index]
        widened = current.astype(jnp.float32)
        squares = lax.psum(jnp.sum(widened * widened, axis=1), "tp")
        inv_rms = lax.rsqrt(squares / D + epsilon)[:, None]
        own_gain = lax.dynamic_slice_in_dim(gain_row, tp_index * feature_part, feature_part)
        normed = (widened * inv_rms * own_gain).astype(jnp.bfloat16)
        partials = jnp.dot(normed, in_all[layer_index], preferred_element_type=jnp.float32)
        pool_in = lax.psum_scatter(
            partials.astype(jnp.bfloat16), "tp", scatter_dimension=1, tiled=True
        )
        edge_block = from_behind(pool_in[row_count - halo_rows :], "sp", 1)
        extended = jnp.concatenate([edge_block, pool_in], 0).astype(jnp.float32)
        means = window_means(
            extended, row_count, tp_index * channel_part, sp_index * row_count, P_SIZE
        )
        own_scale = lax.dynamic_slice_in_dim(
            pool_scale[layer_index], tp_index * channel_part, channel_part
        )
        mixed = (means * own_scale).astype(jnp.bfloat16)
        all_pooled = lax.all_gather(mixed, "tp", axis=1, tiled=True)
        branch = jnp.dot(all_pooled, out_all[layer_index], preferred_element_type=jnp.float32)
        current = (current.astype(jnp.float32) + branch).astype(jnp.bfloat16)
    return current


def solution(mesh):
    placed = (P("sp", "tp"), P(), P(None, "tp", "sp"), P(), P(None, "sp", "tp"))
    return jax.shard_map(body, mesh=mesh, in_specs=placed, out_specs=P("sp", "tp"), check_vma=False)
```

profile of v0, /device:TPU:4, one launch (start us, length us, event | category | flops | bytes accessed | tf_op | source)
XLA Modules:
  0.0 327.6 jit_solution(14062841679788952662)
XLA Ops:
  6.5 0.0 all-gather.3.cloned.1.call-start
  6.5 0.7 all-gather.3.cloned.1.call-update
  7.3 0.0 reduce-scatter.4.cloned.1.call-start
  7.3 1.5 fusion.9
  8.8 4.9 %psum.21 = f32[256]{0:T(256)S(1)} all-reduce(f32[256]{0:T(256)S(1)} %fusion.9), channel_id=1, replica_groups=mesh['sp'=16,'tp'=2] {'tp'}, use_global_device_ids=true, to_apply=%region_1.0 | all-reduce | flops 256 | bytes 2048 | tf_op jit(solution)/shard_map/psum | solution.py:47
  13.8 1.0 fusion.91
  14.8 95.5 %all-gather.3.cloned.1.call-done = bf16[3,2048,1024]{1,2,0:T(8,128)(2,1)} async-done(((bf16[3,2048,64]{1,2,0:T(8,128)(2,1)}), bf16[3,2048,1024]{1,2,0:T(8,128)(2,1)}) %all-gather.3.cloned.1.call-update) | async-done | bytes 12582928 | tf_op jit(solution)/shard_map/all_gather | solution.py:41
  110.3 0.0 copy-start.1
  110.3 4.6 %fusion.18 = bf16[256,1024]{1,0:T(8,128)(2,1)} fusion(bf16[3,2048,1024]{1,2,0:T(8,128)(2,1)} %all-gather.3.cloned.1.call-done, bf16[256,2048]{1,0:T(8,128)(2,1)} %param.5, f32[2048]{0:T(1024)S(1)} %bitcast.54, f32[256]{0:T(256)S(1)} %add_rsqrt_fusion.2), kind=kOutput, calls=%fused_computation.33 | convolution fusion | flops 1076101120 | bytes 5776384 | tf_op jit(solution)/shard_map/dot_general | solution.py:51
  114.9 0.0 reduce-scatter.4.cloned.1.call-update
  114.9 0.0 all-gather.5.cloned.1.call-start
  115.0 0.7 all-gather.5.cloned.1.call-update
  115.7 0.0 reduce-scatter.6.cloned.1.call-start
  115.9 0.0 copy-done.1
  116.0 12.9 %reduce-scatter.4.cloned.1.call-done = bf16[256,512]{1,0:T(8,128)(2,1)} async-done(((bf16[256,1024]{1,0:T(8,128)(2,1)}), bf16[256,512]{1,0:T(8,128)(2,1)}) %reduce-scatter.4.cloned.1.call-update) | async-done | bytes 262160 | tf_op jit(solution)/shard_map/reduce_scatter | solution.py:52
  128.9 0.7 slice.256
  129.6 1.9 collective-permute-start
  131.5 3.1 collective-permute-done
  134.6 1.0 maximum_convert_fusion
  135.6 0.0 copy-start
  135.7 1.2 fusion.84
  136.8 8.2 %all_gather.16 = bf16[256,1024]{1,0:T(8,128)(2,1)S(1)} all-gather(bf16[256,512]{1,0:T(8,128)(2,1)S(1)} %fusion.84), channel_id=1, replica_groups=mesh['sp'=16,'tp'=2] {'tp'}, dimensions={1}, use_global_device_ids=true | all-gather | bytes 786432 | tf_op jit(solution)/shard_map/all_gather | solution.py:64
  145.0 85.6 %all-gather.5.cloned.1.call-done = bf16[3,1024,2048]{2,1,0:T(8,128)(2,1)} async-done(((bf16[3,64,2048]{2,1,0:T(8,128)(2,1)}), bf16[3,1024,2048]{2,1,0:T(8,128)(2,1)}) %all-gather.5.cloned.1.call-update) | async-done | bytes 12582928 | tf_op jit(solution)/shard_map/all_gather | solution.py:42
  230.6 0.0 copy-done
  230.6 3.6 %fusion.12 = (f32[256]{0:T(256)S(1)}, bf16[256,2048]{1,0:T(8,128)(2,1)S(1)}) fusion(bf16[256,1024]{1,0:T(8,128)(2,1)S(1)} %all_gather.16, bf16[3,1024,2048]{2,1,0:T(8,128)(2,1)} %all-gather.5.cloned.1.call-done, bf16[256,2048]{1,0:T(8,128)(2,1)S(1)} %copy-done), kind=kOutput, calls=%fused_computation.27 | convolution fusion | flops 1076887296 | bytes 6816768 | tf_op jit(solution)/shard_map/dot_general | solution.py:65
  234.3 4.9 %psum.22 = f32[256]{0:T(256)S(1)} all-reduce(f32[256]{0:T(256)S(1)} %get-tuple-element.11), channel_id=1, replica_groups=mesh['sp'=16,'tp'=2] {'tp'}, use_global_device_ids=true, to_apply=%region_4.5 | all-reduce | flops 256 | bytes 2048 | tf_op jit(solution)/shard_map/psum | solution.py:47
  239.2 4.3 %fusion.19 = bf16[256,1024]{1,0:T(8,128)(2,1)} fusion(bf16[3,2048,1024]{1,2,0:T(8,128)(2,1)} %all-gather.3.cloned.1.call-done, bf16[256,2048]{1,0:T(8,128)(2,1)S(1)} %get-tuple-element.12, f32[2048]{0:T(1024)S(1)} %bitcast.52, f32[256]{0:T(256)S(1)} %add_rsqrt_fusion.1), kind=kOutput, calls=%fused_computation.34 | convolution fusion | flops 1076101120 | bytes 5776384 | tf_op jit(solution)/shard_map/dot_general | solution.py:51
  243.5 0.0 reduce-scatter.6.cloned.1.call-update
  243.5 0.0 reduce-scatter.8.cloned.1.call-start
  243.6 13.9 %reduce-scatter.6.cloned.1.call-done = bf16[256,512]{1,0:T(8,128)(2,1)} async-done(((bf16[256,1024]{1,0:T(8,128)(2,1)}), bf16[256,512]{1,0:T(8,128)(2,1)}) %reduce-scatter.6.cloned.1.call-update) | async-done | bytes 262160 | tf_op jit(solution)/shard_map/reduce_scatter | solution.py:52
  257.5 0.7 slice.275
  258.2 1.9 collective-permute-start.1
  260.1 3.1 collective-permute-done.1
  263.2 1.0 maximum_convert_fusion.1
  264.2 1.2 fusion.85
  265.4 8.2 %all_gather.18 = bf16[256,1024]{1,0:T(8,128)(2,1)S(1)} all-gather(bf16[256,512]{1,0:T(8,128)(2,1)S(1)} %fusion.85), channel_id=1, replica_groups=mesh['sp'=16,'tp'=2] {'tp'}, dimensions={1}, use_global_device_ids=true | all-gather | bytes 786432 | tf_op jit(solution)/shard_map/all_gather | solution.py:64
  273.6 3.7 %fusion.15 = (f32[256]{0:T(256)S(1)}, bf16[256,2048]{1,0:T(8,128)(2,1)S(1)}) fusion(bf16[256,1024]{1,0:T(8,128)(2,1)S(1)} %all_gather.18, bf16[3,1024,2048]{2,1,0:T(8,128)(2,1)} %all-gather.5.cloned.1.call-done, bf16[256,2048]{1,0:T(8,128)(2,1)S(1)} %get-tuple-element.12), kind=kOutput, calls=%fused_computation.30 | convolution fusion | flops 1076887296 | bytes 6816768 | tf_op jit(solution)/shard_map/dot_general | solution.py:65
  277.2 4.9 %psum.23 = f32[256]{0:T(256)S(1)} all-reduce(f32[256]{0:T(256)S(1)} %get-tuple-element.13), channel_id=1, replica_groups=mesh['sp'=16,'tp'=2] {'tp'}, use_global_device_ids=true, to_apply=%region_7.8 | all-reduce | flops 256 | bytes 2048 | tf_op jit(solution)/shard_map/psum | solution.py:47
  282.2 4.4 %fusion.20 = bf16[256,1024]{1,0:T(8,128)(2,1)} fusion(bf16[3,2048,1024]{1,2,0:T(8,128)(2,1)} %all-gather.3.cloned.1.call-done, bf16[256,2048]{1,0:T(8,128)(2,1)S(1)} %get-tuple-element.14, f32[2048]{0:T(1024)S(1)} %bitcast.53, f32[256]{0:T(256)S(1)} %add_rsqrt_fusion), kind=kOutput, calls=%fused_computation.35 | convolution fusion | flops 1076101120 | bytes 5776384 | tf_op jit(solution)/shard_map/dot_general | solution.py:51
  286.6 0.0 reduce-scatter.8.cloned.1.call-update
  286.6 13.9 %reduce-scatter.8.cloned.1.call-done = bf16[256,512]{1,0:T(8,128)(2,1)} async-done(((bf16[256,1024]{1,0:T(8,128)(2,1)}), bf16[256,512]{1,0:T(8,128)(2,1)}) %reduce-scatter.8.cloned.1.call-update) | async-done | bytes 262160 | tf_op jit(solution)/shard_map/reduce_scatter | solution.py:52
  300.5 0.7 slice.294
  301.2 1.9 collective-permute-start.2
  303.1 3.1 collective-permute-done.2
  306.3 1.0 maximum_convert_fusion.2
  307.3 1.2 fusion.86
  308.5 8.2 %all_gather.19 = bf16[256,1024]{1,0:T(8,128)(2,1)S(1)} all-gather(bf16[256,512]{1,0:T(8,128)(2,1)S(1)} %fusion.86), channel_id=1, replica_groups=mesh['sp'=16,'tp'=2] {'tp'}, dimensions={1}, use_global_device_ids=true | all-gather | bytes 786432 | tf_op jit(solution)/shard_map/all_gather | solution.py:64
  316.6 4.4 %fusion.8 = bf16[256,2048]{1,0:T(8,128)(2,1)} fusion(bf16[256,1024]{1,0:T(8,128)(2,1)S(1)} %all_gather.19, bf16[3,1024,2048]{2,1,0:T(8,128)(2,1)} %all-gather.5.cloned.1.call-done, bf16[256,2048]{1,0:T(8,128)(2,1)S(1)} %get-tuple-element.14), kind=kOutput, calls=%fused_computation.23 | convolution fusion | flops 1075314688 | bytes 6815744 | tf_op jit(solution)/shard_map/dot_general | solution.py:65
  (20 shorter events, 0.2 us)
Async XLA Ops:
  6.5 103.8 %all-gather.3.cloned.1.call-start = ((), (), s32[]{:S(2)}) async-start(), calls=%async_computation.3 | async-start | bytes 13369344 | tf_op jit(solution)/shard_map/all_gather | solution.py:41
  7.3 121.6 %reduce-scatter.4.cloned.1.call-start = ((), (), s32[]{:S(2)}) async-start(), calls=%async_computation.4 | async-start | bytes 786432 | tf_op jit(solution)/shard_map/reduce_scatter | solution.py:52
  110.3 5.6 %copy-start.1 = (f32[3,1024]{1,0:T(4,128)S(1)}, f32[3,1024]{1,0:T(4,128)}, u32[]{:S(2)}) copy-start(f32[3,1024]{1,0:T(4,128)} %param.8) | copy-start | bytes 36868
  114.9 115.7 %all-gather.5.cloned.1.call-start = ((), (), s32[]{:S(2)}) async-start(), calls=%async_computation.5 | async-start | bytes 13369344 | tf_op jit(solution)/shard_map/all_gather | solution.py:42
  115.7 141.8 %reduce-scatter.6.cloned.1.call-start = ((), (), s32[]{:S(2)}) async-start(), calls=%async_computation.6 | async-start | bytes 786432 | tf_op jit(solution)/shard_map/reduce_scatter | solution.py:52
  129.6 5.0 %collective-permute-start = (bf16[16,512]{1,0:T(8,128)(2,1)S(1)}, bf16[16,512]{1,0:T(8,128)(2,1)S(1)}, u32[]{:S(2)}, u32[]{:S(2)}) collective-permute-start(bf16[16,512]{1,0:T(8,128)(2,1)S(1)} %slice.256), channel_id=1, source_target_pairs={{0,2},{2,4},{4,6},{6,8},{8,10},{10,12},{12,14},{14,16},{16,18},{18... | collective-permute-start | bytes 49160 | tf_op jit(solution)/shard_map/ppermute | solution.py:17
  135.6 95.0 %copy-start = (bf16[256,2048]{1,0:T(8,128)(2,1)S(1)}, bf16[256,2048]{1,0:T(8,128)(2,1)}, u32[]{:S(2)}) copy-start(bf16[256,2048]{1,0:T(8,128)(2,1)} %param.5) | copy-start | bytes 3145732
  243.5 57.0 %reduce-scatter.8.cloned.1.call-start = ((), (), s32[]{:S(2)}) async-start(), calls=%async_computation.7 | async-start | bytes 786432 | tf_op jit(solution)/shard_map/reduce_scatter | solution.py:52
  258.2 5.0 %collective-permute-start.1 = (bf16[16,512]{1,0:T(8,128)(2,1)S(1)}, bf16[16,512]{1,0:T(8,128)(2,1)S(1)}, u32[]{:S(2)}, u32[]{:S(2)}) collective-permute-start(bf16[16,512]{1,0:T(8,128)(2,1)S(1)} %slice.275), channel_id=1, source_target_pairs={{0,2},{2,4},{4,6},{6,8},{8,10},{10,12},{12,14},{14,16},{16,18},{18... | collective-permute-start | bytes 49160 | tf_op jit(solution)/shard_map/ppermute | solution.py:17
  301.2 5.0 %collective-permute-start.2 = (bf16[16,512]{1,0:T(8,128)(2,1)S(1)}, bf16[16,512]{1,0:T(8,128)(2,1)S(1)}, u32[]{:S(2)}, u32[]{:S(2)}) collective-permute-start(bf16[16,512]{1,0:T(8,128)(2,1)S(1)} %slice.294), channel_id=1, source_target_pairs={{0,2},{2,4},{4,6},{6,8},{8,10},{10,12},{12,14},{14,16},{16,18},{18... | collective-permute-start | bytes 49160 | tf_op jit(solution)/shard_map/ppermute | solution.py:17
Sparse Core Ops, SparseCore 0:
  9.5 100.7 all-gather.2
  115.1 13.7 reduce-scatter.3
  131.1 99.5 all-gather.4
  243.7 13.7 reduce-scatter.5
  286.7 13.7 reduce-scatter.7
where the time goes:
time: 328 us
  waiting for transfers between devices  233 us (71%)
  blocking collectives  39.3 us (12%)
  matrix products  25 us (8%)
  between operations  13.3 us (4%)
  other arithmetic  8.23 us (3%)
  starting transfers between devices  5.89 us (2%)
    all_gather x1, waiting for transfers between devices, body(): lax.all_gather(in_weight, 'sp', axis=2, tiled=True)  95.5 us
    all_gather x1, waiting for transfers between devices, body(): lax.all_gather(out_weight, 'sp', axis=1, tiled=True)  85.6 us
    reduce_scatter x3, waiting for transfers between devices, body(): lax.psum_scatter(partials.astype(jnp.bfloat16), 'tp', scatter_dimension=1...  40.7 us
    all_gather x3, blocking collectives, body(): all_pooled = lax.all_gather(mixed, 'tp', axis=1, tiled=True)  24.5 us
    psum x3, blocking collectives, body(): squares = lax.psum(jnp.sum(widened * widened, axis=1), 'tp')  14.8 us
    dot_general x3, matrix products, body(): jnp.dot(normed, in_all[layer_index], preferred_element_type=jnp.float32)  13.3 us
    dot_general x3, matrix products, body(): jnp.dot(all_pooled, out_all[layer_index], preferred_element_type=jnp.floa...  11.7 us
    ppermute x3, waiting for transfers between devices, from_behind(): lax.ppermute(value, axis, [(source, source + steps) for source in range(i...  9.34 us
  transfers between devices with their start and end apart: 8, of which 8 were waited for; matrix products, arithmetic and copies ran while one was open for 2% of the time, Pallas kernels for 0%

commit v1 on v0

--- a/solution.py
+++ b/solution.py
@@ -38,7 +38,7 @@
     sp_index = lax.axis_index("sp")
     current = inputs
     in_all, out_all = (
-        lax.all_gather(in_weight, "sp", axis=2, tiled=True),
+        jnp.concatenate(lax.all_gather(in_weight, "sp"), axis=2),
         lax.all_gather(out_weight, "sp", axis=1, tiled=True),
     )
     for layer_index in range(LAYERS):

time: 328 us -> 334 us (1.018)
  local copies, waits for them, and re-layouts: 3.24 us -> 11.1 us
    slice x0 -> x1, local copies, waits for them, and re-layouts: none -> 7.9 us  [body(): in_all[layer_index]]
where the time goes in v1:
time: 334 us; the launch traced here: 333 us
  waiting for transfers between devices  233 us (70%)
  blocking collectives  39.3 us (12%)
  matrix products  22.4 us (7%)
  between operations  13.3 us (4%)
  local copies, waits for them, and re-layouts  11.1 us (3%)
  other arithmetic  8.24 us (2%)
  starting transfers between devices  5.89 us (2%)
    all_gather x1, waiting for transfers between devices, body(): lax.all_gather(in_weight, 'sp')  95.6 us
    all_gather x1, waiting for transfers between devices, body(): lax.all_gather(out_weight, 'sp', axis=1, tiled=True)  85.6 us
    reduce_scatter x3, waiting for transfers between devices, body(): lax.psum_scatter(partials.astype(jnp.bfloat16), 'tp', scatter_dimension=1...  40.7 us
    all_gather x3, blocking collectives, body(): all_pooled = lax.all_gather(mixed, 'tp', axis=1, tiled=True)  24.5 us
    psum x3, blocking collectives, body(): squares = lax.psum(jnp.sum(widened * widened, axis=1), 'tp')  14.8 us
    dot_general x3, matrix products, body(): jnp.dot(all_pooled, out_all[layer_index], preferred_element_type=jnp.floa...  11.7 us
    dot_general x3, matrix products, body(): jnp.dot(normed, in_all[layer_index], preferred_element_type=jnp.float32)  10.7 us
    ppermute x3, waiting for transfers between devices, from_behind(): lax.ppermute(value, axis, [(source, source + steps) for source in range(i...  9.34 us
  transfers between devices with their start and end apart: 8, of which 8 were waited for; matrix products, arithmetic and copies ran while one was open for 2% of the time, Pallas kernels for 0%

profile of v1, /device:TPU:4, one launch (start us, length us, event | category | flops | bytes accessed | tf_op | source)
XLA Modules:
  0.0 333.0 jit_solution(14546295284423887629)
XLA Ops:
  6.5 0.0 all-gather.6.cloned.1.call-start
  6.5 0.7 all-gather.6.cloned.1.call-update
  7.3 0.0 reduce-scatter.4.cloned.1.call-start
  7.3 1.5 fusion.6
  8.8 4.9 %psum.21 = f32[256]{0:T(256)S(1)} all-reduce(f32[256]{0:T(256)S(1)} %fusion.6), channel_id=1, replica_groups=mesh['sp'=16,'tp'=2] {'tp'}, use_global_device_ids=true, to_apply=%region_1.0 | all-reduce | flops 256 | bytes 2048 | tf_op jit(solution)/shard_map/psum | solution.py:47
  13.8 1.0 fusion.86
  14.8 95.6 %all-gather.6.cloned.1.call-done = bf16[48,2048,64]{1,2,0:T(8,128)(2,1)} async-done(((bf16[3,2048,64]{1,2,0:T(8,128)(2,1)}), bf16[48,2048,64]{1,2,0:T(8,128)(2,1)}) %all-gather.6.cloned.1.call-update) | async-done | bytes 12582928 | tf_op jit(solution)/shard_map/all_gather | solution.py:41
  110.4 0.0 copy-start
  110.4 7.9 %fusion.85 = (bf16[1,2048,16,64]{1,3,0,2:T(8,128)(2,1)S(1)}, bf16[1,2048,16,64]{1,3,0,2:T(8,128)(2,1)}, bf16[1,2048,16,64]{1,3,0,2:T(8,128)(2,1)}) fusion(bf16[3,2048,16,64]{1,3,0,2:T(8,128)(2,1)} %bitcast.43), kind=kLoop, calls=%fused_computation.177 | loop fusion | bytes 25165824 | tf_op jit(solution)/shard_map/slice | solution.py:51
  118.3 0.0 copy-done
  118.3 0.0 copy-start.1
  118.3 2.1 convolution_convert_fusion.2
  120.4 0.0 reduce-scatter.4.cloned.1.call-update
  120.4 0.0 all-gather.4.cloned.1.call-start
  120.4 0.7 all-gather.4.cloned.1.call-update
  121.1 0.0 reduce-scatter.6.cloned.1.call-start
  121.3 0.0 copy-done.1
  121.4 12.9 %reduce-scatter.4.cloned.1.call-done = bf16[256,512]{1,0:T(8,128)(2,1)} async-done(((bf16[256,1024]{1,0:T(8,128)(2,1)}), bf16[256,512]{1,0:T(8,128)(2,1)}) %reduce-scatter.4.cloned.1.call-update) | async-done | bytes 262160 | tf_op jit(solution)/shard_map/reduce_scatter | solution.py:52
  134.3 0.7 slice.259
  135.1 1.9 collective-permute-start
  137.0 3.1 collective-permute-done
  140.1 1.0 maximum_convert_fusion
  141.1 1.2 fusion.78
  142.3 8.2 %all_gather.20 = bf16[256,1024]{1,0:T(8,128)(2,1)S(1)} all-gather(bf16[256,512]{1,0:T(8,128)(2,1)S(1)} %fusion.78), channel_id=1, replica_groups=mesh['sp'=16,'tp'=2] {'tp'}, dimensions={1}, use_global_device_ids=true | all-gather | bytes 786432 | tf_op jit(solution)/shard_map/all_gather | solution.py:64
  150.5 85.6 %all-gather.4.cloned.1.call-done = bf16[3,1024,2048]{2,1,0:T(8,128)(2,1)} async-done(((bf16[3,64,2048]{2,1,0:T(8,128)(2,1)}), bf16[3,1024,2048]{2,1,0:T(8,128)(2,1)}) %all-gather.4.cloned.1.call-update) | async-done | bytes 12582928 | tf_op jit(solution)/shard_map/all_gather | solution.py:42
  236.1 3.6 %fusion.9 = (f32[256]{0:T(256)S(1)}, bf16[256,2048]{1,0:T(8,128)(2,1)S(1)}) fusion(bf16[256,1024]{1,0:T(8,128)(2,1)S(1)} %all_gather.20, bf16[3,1024,2048]{2,1,0:T(8,128)(2,1)} %all-gather.4.cloned.1.call-done, bf16[256,2048]{1,0:T(8,128)(2,1)S(1)} %copy-done), kind=kOutput, calls=%fused_computation.21 | convolution fusion | flops 1076887296 | bytes 6816768 | tf_op jit(solution)/shard_map/dot_general | solution.py:65
  239.7 4.9 %psum.22 = f32[256]{0:T(256)S(1)} all-reduce(f32[256]{0:T(256)S(1)} %get-tuple-element.14), channel_id=1, replica_groups=mesh['sp'=16,'tp'=2] {'tp'}, use_global_device_ids=true, to_apply=%region_4.5 | all-reduce | flops 256 | bytes 2048 | tf_op jit(solution)/shard_map/psum | solution.py:47
  244.6 4.3 %convolution_convert_fusion.1 = bf16[256,1024]{1,0:T(8,128)(2,1)} fusion(bf16[2048,1024]{0,1:T(8,128)(2,1)} %bitcast.45, bf16[256,2048]{1,0:T(8,128)(2,1)S(1)} %get-tuple-element.15, f32[2048]{0:T(1024)S(1)} %bitcast.50, f32[256]{0:T(256)S(1)} %add_rsqrt_fusion.1), kind=kOutput, calls=%fused_computation.28 | convolution fusion | flops 1076101120 | bytes 5776384 | tf_op jit(solution)/shard_map/dot_general | solution.py:51
  248.9 0.0 reduce-scatter.6.cloned.1.call-update
  248.9 0.0 reduce-scatter.8.cloned.1.call-start
  249.0 13.9 %reduce-scatter.6.cloned.1.call-done = bf16[256,512]{1,0:T(8,128)(2,1)} async-done(((bf16[256,1024]{1,0:T(8,128)(2,1)}), bf16[256,512]{1,0:T(8,128)(2,1)}) %reduce-scatter.6.cloned.1.call-update) | async-done | bytes 262160 | tf_op jit(solution)/shard_map/reduce_scatter | solution.py:52
  262.9 0.7 slice.278
  263.6 1.9 collective-permute-start.1
  265.6 3.1 collective-permute-done.1
  268.7 1.0 maximum_convert_fusion.1
  269.7 1.2 fusion.79
  270.9 8.2 %all_gather.22 = bf16[256,1024]{1,0:T(8,128)(2,1)S(1)} all-gather(bf16[256,512]{1,0:T(8,128)(2,1)S(1)} %fusion.79), channel_id=1, replica_groups=mesh['sp'=16,'tp'=2] {'tp'}, dimensions={1}, use_global_device_ids=true | all-gather | bytes 786432 | tf_op jit(solution)/shard_map/all_gather | solution.py:64
  279.0 3.7 %fusion.12 = (f32[256]{0:T(256)S(1)}, bf16[256,2048]{1,0:T(8,128)(2,1)S(1)}) fusion(bf16[256,1024]{1,0:T(8,128)(2,1)S(1)} %all_gather.22, bf16[3,1024,2048]{2,1,0:T(8,128)(2,1)} %all-gather.4.cloned.1.call-done, bf16[256,2048]{1,0:T(8,128)(2,1)S(1)} %get-tuple-element.15), kind=kOutput, calls=%fused_computation.24 | convolution fusion | flops 1076887296 | bytes 6816768 | tf_op jit(solution)/shard_map/dot_general | solution.py:65
  282.7 4.9 %psum.23 = f32[256]{0:T(256)S(1)} all-reduce(f32[256]{0:T(256)S(1)} %get-tuple-element.16), channel_id=1, replica_groups=mesh['sp'=16,'tp'=2] {'tp'}, use_global_device_ids=true, to_apply=%region_7.8 | all-reduce | flops 256 | bytes 2048 | tf_op jit(solution)/shard_map/psum | solution.py:47
  287.6 4.3 %convolution_convert_fusion = bf16[256,1024]{1,0:T(8,128)(2,1)} fusion(bf16[2048,1024]{0,1:T(8,128)(2,1)} %bitcast.44, bf16[256,2048]{1,0:T(8,128)(2,1)S(1)} %get-tuple-element.17, f32[2048]{0:T(1024)S(1)} %bitcast.51, f32[256]{0:T(256)S(1)} %add_rsqrt_fusion), kind=kOutput, calls=%fused_computation.27 | convolution fusion | flops 1076101120 | bytes 5776384 | tf_op jit(solution)/shard_map/dot_general | solution.py:51
  291.9 0.0 reduce-scatter.8.cloned.1.call-update
  291.9 13.9 %reduce-scatter.8.cloned.1.call-done = bf16[256,512]{1,0:T(8,128)(2,1)} async-done(((bf16[256,1024]{1,0:T(8,128)(2,1)}), bf16[256,512]{1,0:T(8,128)(2,1)}) %reduce-scatter.8.cloned.1.call-update) | async-done | bytes 262160 | tf_op jit(solution)/shard_map/reduce_scatter | solution.py:52
  305.9 0.7 slice.297
  306.6 1.9 collective-permute-start.2
  308.5 3.1 collective-permute-done.2
  311.6 1.0 maximum_convert_fusion.2
  312.6 1.2 fusion.80
  313.8 8.2 %all_gather.23 = bf16[256,1024]{1,0:T(8,128)(2,1)S(1)} all-gather(bf16[256,512]{1,0:T(8,128)(2,1)S(1)} %fusion.80), channel_id=1, replica_groups=mesh['sp'=16,'tp'=2] {'tp'}, dimensions={1}, use_global_device_ids=true | all-gather | bytes 786432 | tf_op jit(solution)/shard_map/all_gather | solution.py:64
  322.0 4.5 %fusion.5 = bf16[256,2048]{1,0:T(8,128)(2,1)} fusion(bf16[256,1024]{1,0:T(8,128)(2,1)S(1)} %all_gather.23, bf16[3,1024,2048]{2,1,0:T(8,128)(2,1)} %all-gather.4.cloned.1.call-done, bf16[256,2048]{1,0:T(8,128)(2,1)S(1)} %get-tuple-element.17), kind=kOutput, calls=%fused_computation.17 | convolution fusion | flops 1075314688 | bytes 6815744 | tf_op jit(solution)/shard_map/dot_general | solution.py:65
  (20 shorter events, 0.2 us)
Async XLA Ops:
  6.5 103.8 %all-gather.6.cloned.1.call-start = ((), (), s32[]{:S(2)}) async-start(), calls=%async_computation.7 | async-start | bytes 13369344 | tf_op jit(solution)/shard_map/all_gather | solution.py:41
  7.3 127.1 %reduce-scatter.4.cloned.1.call-start = ((), (), s32[]{:S(2)}) async-start(), calls=%async_computation.3 | async-start | bytes 786432 | tf_op jit(solution)/shard_map/reduce_scatter | solution.py:52
  110.4 7.9 %copy-start = (bf16[256,2048]{1,0:T(8,128)(2,1)S(1)}, bf16[256,2048]{1,0:T(8,128)(2,1)}, u32[]{:S(2)}) copy-start(bf16[256,2048]{1,0:T(8,128)(2,1)} %param.5) | copy-start | bytes 3145732
  118.3 3.1 copy-start.1
  120.4 115.7 %all-gather.4.cloned.1.call-start = ((), (), s32[]{:S(2)}) async-start(), calls=%async_computation.4 | async-start | bytes 13369344 | tf_op jit(solution)/shard_map/all_gather | solution.py:42
  121.1 141.8 %reduce-scatter.6.cloned.1.call-start = ((), (), s32[]{:S(2)}) async-start(), calls=%async_computation.5 | async-start | bytes 786432 | tf_op jit(solution)/shard_map/reduce_scatter | solution.py:52
  135.1 5.0 %collective-permute-start = (bf16[16,512]{1,0:T(8,128)(2,1)S(1)}, bf16[16,512]{1,0:T(8,128)(2,1)S(1)}, u32[]{:S(2)}, u32[]{:S(2)}) collective-permute-start(bf16[16,512]{1,0:T(8,128)(2,1)S(1)} %slice.259), channel_id=1, source_target_pairs={{0,2},{2,4},{4,6},{6,8},{8,10},{10,12},{12,14},{14,16},{16,18},{18... | collective-permute-start | bytes 49160 | tf_op jit(solution)/shard_map/ppermute | solution.py:17
  248.9 56.9 %reduce-scatter.8.cloned.1.call-start = ((), (), s32[]{:S(2)}) async-start(), calls=%async_computation.6 | async-start | bytes 786432 | tf_op jit(solution)/shard_map/reduce_scatter | solution.py:52
  263.6 5.0 %collective-permute-start.1 = (bf16[16,512]{1,0:T(8,128)(2,1)S(1)}, bf16[16,512]{1,0:T(8,128)(2,1)S(1)}, u32[]{:S(2)}, u32[]{:S(2)}) collective-permute-start(bf16[16,512]{1,0:T(8,128)(2,1)S(1)} %slice.278), channel_id=1, source_target_pairs={{0,2},{2,4},{4,6},{6,8},{8,10},{10,12},{12,14},{14,16},{16,18},{18... | collective-permute-start | bytes 49160 | tf_op jit(solution)/shard_map/ppermute | solution.py:17
  306.6 5.0 %collective-permute-start.2 = (bf16[16,512]{1,0:T(8,128)(2,1)S(1)}, bf16[16,512]{1,0:T(8,128)(2,1)S(1)}, u32[]{:S(2)}, u32[]{:S(2)}) collective-permute-start(bf16[16,512]{1,0:T(8,128)(2,1)S(1)} %slice.297), channel_id=1, source_target_pairs={{0,2},{2,4},{4,6},{6,8},{8,10},{10,12},{12,14},{14,16},{16,18},{18... | collective-permute-start | bytes 49160 | tf_op jit(solution)/shard_map/ppermute | solution.py:17
Sparse Core Ops, SparseCore 0:
  9.6 100.6 all-gather.5
  120.5 13.7 reduce-scatter.3
  136.5 99.5 all-gather.3
  249.1 13.7 reduce-scatter.5
  292.1 13.7 reduce-scatter.7
